TPU v7x, 32 devices: a whole 2x2x4 slice. The times are simulated.
32 devices in a mesh: grp: 2 (over y), row: 4 (over z), col: 4 (over x, core).
Axes of the slice: x: 2, y: 2, z: 4, core: 2. Of those that a mesh axis runs over, the one named last changes fastest.
Arguments:
- tokens: bfloat16 [2048, 2048], P(('grp', 'row')), parts along dimension 0, may hold values from -6 to 6
- w_value: bfloat16 [2048, 2048], P(None, 'col'), may hold values from -0.125 to 0.125
- w_gate_a: bfloat16 [2048, 2048], P(None, 'col'), may hold values from -0.125 to 0.125
- w_gate_b: bfloat16 [2048, 2048], P(None, 'col'), may hold values from -0.125 to 0.125
- short_taps: bfloat16 [3, 3, 2048], replicated, may hold values from -3.5 to 3.5
- pos_weight: float32 [33, 64], replicated, may hold values from -3 to 3
- pos_bias: float32 [64], replicated, may hold values from -3 to 3
- sine_freq: float32 [2, 64], replicated, may hold values from 1.2 to 2
- hid_weight: float32 [64, 64], replicated, may hold values from -1.5 to 1.5
- hid_bias: float32 [64], replicated, may hold values from -3 to 3
- filter_out: float32 [64, 2, 2, 2048], P(None, None, None, 'col'), may hold values from -0.046875 to 0.046875
- filter_bias: float32 [2, 2048], replicated, may hold values from -3 to 3
- lag_decay: float32 [2048], replicated, may hold values from 1 to 35, as said below
Outputs:
- mixed: bfloat16 [2048, 2048], P(('grp', 'row'), 'col'), parts along dimension 0
There are 2 independent parts, one for each index of `grp`. A program takes and returns all parts, laid end to end along the dimension named above; an argument that names none is the same for every part. Nothing has to cross between parts.
Inputs may be any that keep to these rules, and one draw needn't show every extreme that they name: `lag_decay`: each channel's envelope decay is positive.
All inputs are finite; a program needn't handle non-finite values.
Results may differ from a plain program's by a relative error of at most 0.0081.
Values may be sent and summed in bfloat16 or wider, within the bound.
A program may use at most 64 MiB of HBM per device.

v0:
```python
import functools
import math

import jax
import jax.numpy as jnp
import numpy as np
from jax import lax
from jax.experimental import pallas as pl
from jax.experimental.pallas import tpu as pltpu
from jax.sharding import PartitionSpec as P

WINDOW_SHIFT = 0.05
LEAF = 128
CHUNK = 16
MESH = pl.DeviceIdType.MESH
F32 = jnp.float32
BF16 = jnp.bfloat16


def leaf_angles(theta, count):
    if count == 1:
        return [theta]
    half = theta / 2
    return leaf_angles(half, count // 2) + leaf_angles(half + math.pi, count // 2)


def split_np(values):
    high = values.astype(jnp.bfloat16)
    low = (values - high.astype(np.float64)).astype(jnp.bfloat16)
    return high, low


@functools.lru_cache(maxsize=None)
def tables(seq, lanes, features, hidden):
    k = np.arange(LEAF)
    angle = 2 * np.pi / LEAF * ((k[:, None] * k[None, :]) % LEAF)
    cos, sin = np.cos(angle), np.sin(angle)
    forward = np.block([[cos, -sin], [sin, cos]])
    inverse = np.block([[cos, sin], [-sin, cos]]) / seq
    fcat = np.concatenate(split_np(forward), axis=0)
    gcat = np.concatenate(split_np(inverse), axis=0)
    thetas = np.array(leaf_angles(math.pi / 2, seq // LEAF))
    twist = (thetas[:, None] * k[None, :] / LEAF).reshape(-1)
    twist = np.stack([np.cos(twist), np.sin(twist)]).astype(np.float32)
    twist = np.ascontiguousarray(np.broadcast_to(twist[:, :, None], (2, seq, lanes)))
    bands = (features - 1) // 2
    freq = np.linspace(0.0001, bands - 1, bands, dtype=np.float32)

    def feats(positions):
        positions = positions.astype(np.float32)
        scaled = positions / np.float32(max(seq - 1, 1))
        ang = (np.float32(2.0 * math.pi / seq) * positions)[:, None] * freq[None, :]
        ang = ang.astype(np.float64)
        return np.concatenate([scaled[:, None], np.cos(ang), -np.sin(ang)], axis=1)

    both = np.zeros((seq, 2 * hidden))
    both[:, :features] = feats(np.arange(seq))
    both[:, hidden : hidden + features] = feats(seq - np.arange(seq))
    fhi, flo = split_np(both)
    return fcat, gcat, twist, fhi, flo


def split(x):
    high = x.astype(BF16)
    return high, (x - high.astype(F32)).astype(BF16)


def dot(a, b):
    return jnp.dot(a, b, preferred_element_type=F32)


def dot3(a, b):
    return dot(a[0], b[0]) + dot(a[1], b[0]) + dot(a[0], b[1])


PI_A = 3.140625
PI_B = float(np.float32(math.pi - 3.140625))
PI_C = float(math.pi - 3.140625 - np.float32(math.pi - 3.140625))


def sine(x):
    k = jnp.floor(x * (1.0 / math.pi) + 0.5)
    r = x - k * PI_A
    r = r - k * PI_B
    r = r - k * PI_C
    parity = k - 2.0 * jnp.floor(k * 0.5)
    s = r * r
    p = -1.0 / 39916800.0
    for c in (1.0 / 362880.0, -1.0 / 5040.0, 1.0 / 120.0, -1.0 / 6.0):
        p = p * s + c
    return (r + r * s * p) * (1.0 - 2.0 * parity)


def split_tree(blocks, theta):
    if len(blocks) == 1:
        return blocks
    half = len(blocks) // 2
    wr, wi = math.cos(theta / 2), math.sin(theta / 2)
    up, down = [], []
    for (ar, ai), (br, bi) in zip(blocks[:half], blocks[half:]):
        if bi is None:
            tr, ti = br * wr, br * wi
            up.append((ar + tr, ti))
            down.append((ar - tr, -ti))
        else:
            tr, ti = br * wr - bi * wi, br * wi + bi * wr
            up.append((ar + tr, ai + ti))
            down.append((ar - tr, ai - ti))
    return split_tree(up, theta / 2) + split_tree(down, theta / 2 + math.pi)


def join_tree(leaves, theta, top):
    if len(leaves) == 1:
        return leaves
    half = len(leaves) // 2
    up = join_tree(leaves[:half], theta / 2, False)
    down = join_tree(leaves[half:], theta / 2 + math.pi, False)
    wr, wi = math.cos(theta / 2), math.sin(theta / 2)
    first, second = [], []
    for (pr, pi), (qr, qi) in zip(up, down):
        dr, di = pr - qr, pi - qi
        if top:
            first.append(pr + qr)
            second.append(dr * wr + di * wi)
        else:
            first.append((pr + qr, pi + qi))
            second.append((dr * wr + di * wi, di * wr - dr * wi))
    return first + second


def kernel(
    sizes,
    tok_h, wv_h, wa_h, wb_h, fcat_h, gcat_h, twist_h, fhi_h, flo_h,
    wf_h, own_taps_h, gate_taps_h, pw_h, pb_h, sf_h, hw_h, hb_h, fb_h, ld_h,
    out_ref,
    own_taps, gate_taps, pw, pb, sf, hw, hb, fb, ld,
    tok, wva, wb, fcat, gcat, twist, fhi, flo,
    wf, sbuf, rbuf, gb, halo, pad, xs, gs, gpad, gbs,
    pwb, hwb, wfb, kre, kim, xhi, xlo, spec, ybuf, s2, r2,
    in_sem, send_sem, recv_sem, halo_send, halo_recv, back_send, back_recv,
):
    R, T, N, C, S, HID, PE = sizes
    L = N // LEAF
    row = lax.axis_index("row")
    col = lax.axis_index("col")
    aligned = C % 128 == 0
    if aligned:
        own_at = pl.ds(pl.multiple_of(col * S + row * C, 128), C)
        share_at = pl.ds(pl.multiple_of(col * S, 128), S)
    else:
        own_at, share_at = slice(0, C), slice(0, S)

    half = R // 2
    H = S // 2
    far = 1 - row // half
    order = [far, 1 - far]

    def load(i, src, dst):
        copy = pltpu.make_async_copy(src, dst, in_sem.at[i])
        copy.start()
        return copy

    def load_half(i, src, which, k):
        lanes = pl.ds(pl.multiple_of(order[k] * H, H), H)
        return load(i, src.at[:, lanes], wva.at[k, :, which * H : (which + 1) * H])

    ld_tok = load(0, tok_h, tok)
    ld_half = [
        [load_half(2 * k + which + 1, src, which, k) for which, src in enumerate((wv_h, wa_h))]
        for k in range(2)
    ]

    barrier = pltpu.get_barrier_semaphore()
    peers = [lax.rem(row + d, R) for d in range(R)]
    sources = [lax.rem(row + R - d, R) for d in range(R)]
    for d in range(1, R):
        pl.semaphore_signal(barrier, inc=1, device_id={"row": peers[d]}, device_id_type=MESH)

    def out_copy(which, target, slot):
        return pltpu.make_async_remote_copy(
            src_ref=sbuf.at[which, target], dst_ref=rbuf.at[which, row],
            send_sem=send_sem.at[which, slot], recv_sem=recv_sem.at[which, row],
            device_id={"row": target}, device_id_type=MESH)

    def in_copy(which, d):
        return pltpu.make_async_remote_copy(
            src_ref=sbuf.at[which, peers[d]], dst_ref=rbuf.at[which, sources[d]],
            send_sem=send_sem.at[which, d], recv_sem=recv_sem.at[which, sources[d]],
            device_id={"row": peers[d]}, device_id_type=MESH)

    def halo_copy(side):
        src = gb.at[pl.ds(T - CHUNK, CHUNK)] if side == 0 else gb.at[pl.ds(0, CHUNK)]
        target = peers[1] if side == 0 else peers[R - 1]
        return pltpu.make_async_remote_copy(
            src_ref=src, dst_ref=halo.at[side],
            send_sem=halo_send.at[side], recv_sem=halo_recv.at[side],
            device_id={"row": target}, device_id_type=MESH)

    def back_out(d):
        return pltpu.make_async_remote_copy(
            src_ref=s2.at[peers[d]], dst_ref=r2.at[row],
            send_sem=back_send.at[d], recv_sem=back_recv.at[d],
            device_id={"row": peers[d]}, device_id_type=MESH)

    def back_in(d):
        return pltpu.make_async_remote_copy(
            src_ref=s2.at[peers[d]], dst_ref=r2.at[sources[d]],
            send_sem=back_send.at[d], recv_sem=back_recv.at[d],
            device_id={"row": peers[d]}, device_id_type=MESH)

    ld_tok.wait()
    sends = []
    first = lax.rem(row, half)

    def send(which, k):
        for i in range(k, half):
            target = order[k] * half + lax.rem(first + i, half)
            copy = out_copy(which, target, k * half + i)
            copy.start()
            sends.append(copy)

    for k in range(2):
        for copy in ld_half[k]:
            copy.wait()
        if k == 0:
            ld_wb = load(5, wb_h, wb)
            ld_fhi, ld_flo = load(6, fhi_h, fhi), load(7, flo_h, flo)
            small = [
                load(12 + i, src, dst)
                for i, (src, dst) in enumerate([
                    (own_taps_h, own_taps), (gate_taps_h, gate_taps), (pw_h, pw), (pb_h, pb),
                    (sf_h, sf), (hw_h, hw), (hb_h, hb), (fb_h, fb), (ld_h, ld)])
            ]
        made = dot(tok[...], wva[k]).astype(BF16)
        for which in range(2):
            for i in range(half):
                base = which * H + i * C
                sbuf[which, order[k] * half + i] = made[:, base : base + C]
        if k == 0:
            pl.semaphore_wait(barrier, R - 1)
            send(0, 0)
    send(0, 1)
    send(1, 0)
    send(1, 1)
    for which in range(2):
        rbuf[which, row] = sbuf[which, row]
    if aligned:
        wf_src = wf_h.at[:, :, :, pl.ds(pl.multiple_of(row * C, 128), C)]
    else:
        wf_src = wf_h
    ld_wf = load(8, wf_src, wf)
    ld_fcat, ld_twist, ld_gcat = load(9, fcat_h, fcat), load(10, twist_h, twist), load(11, gcat_h, gcat)
    ld_wb.wait()
    gb[...] = dot(tok[...], wb[...]).astype(BF16)
    for side in range(2):
        halo_copy(side).start()

    for copy in small:
        copy.wait()
    pwb[...] = jnp.zeros_like(pwb)
    pwb[0:PE, 0:HID] = pw[...]
    pwb[HID : HID + PE, HID : 2 * HID] = pw[...]
    hwb[...] = jnp.zeros_like(hwb)
    hwb[0:HID, 0:HID] = hw[...]
    hwb[HID : 2 * HID, HID : 2 * HID] = hw[...]
    wfb[...] = jnp.zeros_like(wfb)
    ld_wf.wait()
    for o in range(2):
        wfb[0:HID, o * C : (o + 1) * C] = wf[:, o, 0, :]
        wfb[HID : 2 * HID, (2 + o) * C : (3 + o) * C] = wf[:, o, 1, :]
    ld_fhi.wait()
    ld_flo.wait()

    def twice(v):
        return jnp.concatenate([v, v], axis=-1)

    decay = ld[:, own_at]
    rows_f = 256
    pb2, hb2, sf2 = twice(pb[...]), twice(hb[...]), twice(sf[...])

    def filter_rows(step, carry):
        at = pl.ds(pl.multiple_of(step * rows_f, rows_f), rows_f)
        pre = dot3((fhi[at, :], flo[at, :]), split(pwb[...])) + pb2
        ha = sine(sf2[0:1] * pre)
        pre = dot3(split(ha), split(hwb[...])) + hb2
        hb_ = sine(sf2[1:2] * pre)
        raw = dot3(split(hb_), split(wfb[...]))
        index = (lax.broadcasted_iota(jnp.int32, (rows_f, C), 0) + step * rows_f).astype(F32)
        scale = 1.0 / max(N - 1, 1)
        env_f = jnp.exp(-(index * scale) * decay) + WINDOW_SHIFT
        env_b = jnp.exp(-((N - index) * scale) * decay) + WINDOW_SHIFT
        env_b = jnp.where(index > 0.0, -env_b, 0.0)
        for o in range(2):
            kre[o, at, :] = raw[:, o * C : (o + 1) * C] * env_f
            kim[o, at, :] = raw[:, (2 + o) * C : (3 + o) * C] * env_b
        return carry

    lax.fori_loop(0, N // rows_f, filter_rows, 0)
    ld_fcat.wait()
    ld_twist.wait()
    ld_gcat.wait()

    def put_leaves(leaves, at, exact):
        for j, (re, im) in enumerate(leaves):
            tat = pl.ds(pl.multiple_of(j * LEAF + at, CHUNK), CHUNK)
            tc, ts = twist[0, tat, :], twist[1, tat, :]
            zr, zi = re * tc - im * ts, re * ts + im * tc
            lanes = slice(j * C, (j + 1) * C)
            for part, base in ((zr, 0), (zi, LEAF)):
                pat = pl.ds(pl.multiple_of(base + at, CHUNK), CHUNK)
                if exact:
                    xhi[pat, lanes], xlo[pat, lanes] = split(part)
                else:
                    xhi[pat, lanes] = part.astype(BF16)

    def get_leaves(at):
        leaves = []
        for j in range(L):
            tat = pl.ds(pl.multiple_of(j * LEAF + at, CHUNK), CHUNK)
            tc, ts = twist[0, tat, :], twist[1, tat, :]
            lanes = slice(j * C, (j + 1) * C)
            zr = ybuf[pl.ds(pl.multiple_of(at, CHUNK), CHUNK), lanes]
            zi = ybuf[pl.ds(pl.multiple_of(LEAF + at, CHUNK), CHUNK), lanes]
            leaves.append((zr * tc + zi * ts, zi * tc - zr * ts))
        return leaves

    width = 256 if (L * C) % 256 == 0 else L * C
    K2 = 2 * LEAF

    def mul3(cat, hi, lo):
        both = dot(cat[...], hi)
        return both[:K2] + both[K2:] + dot(cat[0:K2], lo)

    steps = LEAF // CHUNK

    def rows_at(n1, at):
        return pl.ds(pl.multiple_of(n1 * LEAF + at, CHUNK), CHUNK)

    for o in range(2):
        def kernel_in(step, carry, o=o):
            at = step * CHUNK
            blocks = [(kre[o, rows_at(n1, at), :], kim[o, rows_at(n1, at), :]) for n1 in range(L)]
            put_leaves(split_tree(blocks, math.pi / 2), at, True)
            return carry

        lax.fori_loop(0, steps, kernel_in, 0)
        for tile in range(L * C // width):
            lanes = slice(tile * width, (tile + 1) * width)
            spec[o, :, lanes] = mul3(fcat, xhi[:, lanes], xlo[:, lanes])

    def through(o, exact):
        for tile in range(L * C // width):
            lanes = slice(tile * width, (tile + 1) * width)
            if exact:
                z = mul3(fcat, xhi[:, lanes], xlo[:, lanes])
            else:
                z = dot(fcat[0:K2], xhi[:, lanes])
            zr, zi = z[:LEAF], z[LEAF:]
            kr, ki = spec[o, 0:LEAF, lanes], spec[o, LEAF:K2, lanes]
            y = jnp.concatenate([zr * kr - zi * ki, zr * ki + zi * kr], axis=0)
            if exact:
                ybuf[:, lanes] = mul3(gcat, *split(y))
            else:
                ybuf[:, lanes] = dot(gcat[0:K2], y.astype(BF16))

    def short(which, dest):
        for d in range(1, R):
            in_copy(which, d).wait_recv()
        pad[0:8] = jnp.zeros((8, C), F32)
        pad[8 + N : 16 + N] = jnp.zeros((8, C), F32)
        for r in range(R):
            pad[8 + r * T : 8 + (r + 1) * T] = rbuf[which, r].astype(F32)
        taps = own_taps[which, :, own_at].astype(F32)
        for r in range(R):
            a = r * T
            dest[a : a + T] = (
                taps[0:1] * pad[7 + a : 7 + a + T]
                + taps[1:2] * pad[8 + a : 8 + a + T]
                + taps[2:3] * pad[9 + a : 9 + a + T]
            ).astype(BF16).astype(F32)

    short(0, xs)
    bias = fb[:, own_at]

    def value_in(step, carry):
        at = step * CHUNK
        blocks = [(xs[rows_at(n1, at), :], None) for n1 in range(L)]
        put_leaves(split_tree(blocks, math.pi / 2), at, True)
        return carry

    lax.fori_loop(0, steps, value_in, 0)
    through(0, True)
    short(1, gs)

    def middle(step, carry):
        at = step * CHUNK
        convolved = join_tree(get_leaves(at), math.pi / 2, True)
        blocks = []
        for n1 in range(L):
            here = rows_at(n1, at)
            gated = gs[here, :] * (convolved[n1] + bias[0:1] * xs[here, :])
            xs[here, :] = gated
            blocks.append((gated, None))
        put_leaves(split_tree(blocks, math.pi / 2), at, False)
        return carry

    lax.fori_loop(0, steps, middle, 0)
    through(1, False)

    def last(step, carry):
        at = step * CHUNK
        convolved = join_tree(get_leaves(at), math.pi / 2, True)
        for n1 in range(L):
            value = convolved[n1] + bias[1:2] * xs[rows_at(n1, at), :]
            r, inner = (n1 * LEAF) // T, (n1 * LEAF) % T
            s2[r, pl.ds(pl.multiple_of(inner + at, CHUNK), CHUNK), :] = value.astype(BF16)
        return carry

    lax.fori_loop(0, steps, last, 0)
    for d in [half] + [d for d in range(1, R) if d != half]:
        back_out(d).start()
    r2[row] = s2[row]

    for side in range(2):
        halo_copy(side).wait_recv()
    before = halo[0, CHUNK - 8 : CHUNK].astype(F32)
    after = halo[1, 0:8].astype(F32)
    gpad[0:8] = jnp.where(row > 0, before, 0.0)
    gpad[8 : 8 + T] = gb[...].astype(F32)
    gpad[8 + T : 16 + T] = jnp.where(row < R - 1, after, 0.0)
    taps = gate_taps[2, :, share_at].astype(F32)
    gbs[...] = (
        taps[0:1] * gpad[7 : 7 + T] + taps[1:2] * gpad[8 : 8 + T] + taps[2:3] * gpad[9 : 9 + T]
    ).astype(BF16).astype(F32)
    for d in range(1, R):
        back_in(d).wait_recv()
    for r in range(R):
        lanes = slice(r * C, (r + 1) * C)
        out_ref[:, lanes] = (gbs[:, lanes] * r2[r].astype(F32)).astype(BF16)
    for copy in sends:
        copy.wait_send()
    for d in range(1, R):
        back_out(d).wait_send()
    for side in range(2):
        halo_copy(side).wait_send()


def per_device(
    tokens, w_value, w_gate_a, w_gate_b, short_taps, pos_weight, pos_bias, sine_freq,
    hid_weight, hid_bias, filter_out, filter_bias, lag_decay,
):
    R = lax.axis_size("row")
    T, D = tokens.shape
    N = T * R
    S = w_value.shape[1]
    C = S // R
    PE, HID = pos_weight.shape
    L = N // LEAF
    row, col = lax.axis_index("row"), lax.axis_index("col")
    fcat, gcat, twist, fhi, flo = tables(N, C, PE, HID)
    own_w = filter_out
    own_taps, gate_taps, fb, ld = short_taps, short_taps, filter_bias, lag_decay[None]
    if C % 128:
        own_w = lax.dynamic_slice_in_dim(own_w, row * C, C, 3)
        start = col * S + row * C
        own_taps = lax.dynamic_slice_in_dim(own_taps, start, C, 2)
        gate_taps = lax.dynamic_slice_in_dim(gate_taps, col * S, S, 2)
        fb = lax.dynamic_slice_in_dim(fb, start, C, 1)
        ld = lax.dynamic_slice_in_dim(ld, start, C, 1)
    vm = pl.BlockSpec(memory_space=pltpu.VMEM)
    hbm = pl.BlockSpec(memory_space=pl.ANY)
    dma = pltpu.SemaphoreType.DMA
    small = [own_taps, gate_taps, pos_weight, pos_bias[None], sine_freq, hid_weight, hid_bias[None], fb, ld]
    return pl.pallas_call(
        functools.partial(kernel, (R, T, N, C, S, HID, PE)),
        out_shape=jax.ShapeDtypeStruct((T, S), BF16),
        in_specs=[hbm] * 19,
        out_specs=vm,
        scratch_shapes=[pltpu.VMEM(x.shape, x.dtype) for x in small] + [
            pltpu.VMEM((T, D), BF16),
            pltpu.VMEM((2, D, S), BF16),
            pltpu.VMEM((D, S), BF16),
            pltpu.VMEM(fcat.shape, BF16),
            pltpu.VMEM(gcat.shape, BF16),
            pltpu.VMEM(twist.shape, F32),
            pltpu.VMEM(fhi.shape, BF16),
            pltpu.VMEM(flo.shape, BF16),
            pltpu.VMEM((HID, 2, 2, C), F32),
            pltpu.VMEM((2, R, T, C), BF16),
            pltpu.VMEM((2, R, T, C), BF16),
            pltpu.VMEM((T, S), BF16),
            pltpu.VMEM((2, CHUNK, S), BF16),
            pltpu.VMEM((N + 16, C), F32),
            pltpu.VMEM((N, C), F32),
            pltpu.VMEM((N, C), F32),
            pltpu.VMEM((T + 16, S), F32),
            pltpu.VMEM((T, S), F32),
            pltpu.VMEM((2 * HID, 2 * HID), F32),
            pltpu.VMEM((2 * HID, 2 * HID), F32),
            pltpu.VMEM((2 * HID, 4 * C), F32),
            pltpu.VMEM((2, N, C), F32),
            pltpu.VMEM((2, N, C), F32),
            pltpu.VMEM((2 * LEAF, L * C), BF16),
            pltpu.VMEM((2 * LEAF, L * C), BF16),
            pltpu.VMEM((2, 2 * LEAF, L * C), F32),
            pltpu.VMEM((2 * LEAF, L * C), F32),
            pltpu.VMEM((R, T, C), BF16),
            pltpu.VMEM((R, T, C), BF16),
            dma((21,)),
            dma((2, R)),
            dma((2, R)),
            dma((2,)),
            dma((2,)),
            dma((R,)),
            dma((R,)),
        ],
        compiler_params=pltpu.CompilerParams(
            collective_id=0, has_side_effects=True, vmem_limit_bytes=60 * 1024 * 1024
        ),
    )(
        tokens, w_value, w_gate_a, w_gate_b, fcat, gcat, twist, fhi, flo,
        own_w, *small,
    )


def solution(mesh):
    in_specs = (
        P(("grp", "row"), None), P(None, "col"), P(None, "col"), P(None, "col"),
        P(), P(), P(), P(), P(), P(), P(None, None, None, "col"), P(), P(),
    )
    return jax.shard_map(
        per_device, mesh=mesh, in_specs=in_specs, out_specs=P(("grp", "row"), "col"), check_vma=False
    )
```

profile of v0, /device:TPU:0, one launch (start us, length us, event | category | flops | bytes accessed | tf_op | source)
XLA Modules:
  0.0 28.5 jit_solution(12956889433208461393)
XLA Ops:
  0.0 26.8 %shard_map.172 = bf16[256,512]{1,0:T(8,128)(2,1)} custom-call(bf16[256,2048]{1,0:T(8,128)(2,1)} %tok_h.1, bf16[2048,512]{1,0:T(8,128)(2,1)} %wv_h.1, bf16[2048,512]{1,0:T(8,128)(2,1)} %wa_h.1, bf16[2048,512]{1,0:T(8,128)(2,1)} %wb_h.1, bf16[512,256]{1,0:T(8,128)(2,1)} %constant.10.clone.fcat_h, bf16[512,256]{1,0:T(8,128)(2,1)} %constant.11.clone.gcat_h, ...), custom_call_target="tpu_custom_call" | custom-call | tf_op jit(solution)/shard_map/pallas_call | solution.py:474
  26.8 1.7 %copy.20 = bf16[256,512]{1,0:T(8,128)(2,1)} copy(bf16[256,512]{1,0:T(8,128)(2,1)} %shard_map.172) | data formatting | bytes 524288
where the time goes:
time: 28.6 us; the launch traced here: 28.5 us
  Pallas kernels  26.8 us (94%)
  local copies, waits for them, and re-layouts  1.67 us (6%)
    pallas_call x1, Pallas kernels, per_device(): pl.pallas_call(functools.partial(kernel, (R, T, N, C, S, HID, PE)), out_s...  26.8 us
    unnamed x1, local copies, waits for them, and re-layouts  1.67 us

commit v1 on v0

--- a/solution.py
+++ b/solution.py
@@ -515,12 +515,12 @@
             dma((R,)),
         ],
         compiler_params=pltpu.CompilerParams(
-            collective_id=0, has_side_effects=True, vmem_limit_bytes=60 * 1024 * 1024
+            collective_id=0, has_side_effects=True, vmem_limit_bytes=44 * 1024 * 1024
         ),
-    )(
-        tokens, w_value, w_gate_a, w_gate_b, fcat, gcat, twist, fhi, flo,
-        own_w, *small,
-    )
+    )(*[
+        pltpu.with_memory_space_constraint(jnp.asarray(x), pltpu.HBM)
+        for x in (tokens, w_value, w_gate_a, w_gate_b, fcat, gcat, twist, fhi, flo, own_w, *small)
+    ])
 
 
 def solution(mesh):

time: 28.6 us -> 27 us (0.944)
  local copies, waits for them, and re-layouts: 1.67 us -> 0.71 us
  Pallas kernels: 26.8 us -> 26.1 us
    unnamed x1, local copies, waits for them, and re-layouts: 1.67 us -> 0.71 us
    pallas_call x1, Pallas kernels: 26.8 us -> 26.1 us  [per_device(): pl.pallas_call(functools.partial(kernel, (R, T, N, C, S, HID, PE)), out_s...]
where the time goes in v1:
time: 27 us; the launch traced here: 26.8 us
  Pallas kernels  26.1 us (97%)
  local copies, waits for them, and re-layouts  0.71 us (3%)
    pallas_call x1, Pallas kernels, per_device(): pl.pallas_call(functools.partial(kernel, (R, T, N, C, S, HID, PE)), out_s...  26.1 us
    unnamed x1, local copies, waits for them, and re-layouts  0.71 us

profile of v1, /device:TPU:0, one launch (start us, length us, event | category | flops | bytes accessed | tf_op | source)
XLA Modules:
  0.0 26.8 jit_solution(9734311411162298412)
XLA Ops:
  0.0 26.1 %shard_map.172 = bf16[256,512]{1,0:T(8,128)(2,1)S(1)} custom-call(bf16[256,2048]{1,0:T(8,128)(2,1)} %tok_h.1, bf16[2048,512]{1,0:T(8,128)(2,1)} %wv_h.1, bf16[2048,512]{1,0:T(8,128)(2,1)} %wa_h.1, bf16[2048,512]{1,0:T(8,128)(2,1)} %wb_h.1, bf16[512,256]{1,0:T(8,128)(2,1)} %constant.10.clone.fcat_h, bf16[512,256]{1,0:T(8,128)(2,1)} %constant.11.clone.gcat_h, ...), custom_call_target="tpu_custom_call" | custom-call | tf_op jit(solution)/shard_map/pallas_call | solution.py:474
  26.1 0.7 %copy.20 = bf16[256,512]{1,0:T(8,128)(2,1)} copy(bf16[256,512]{1,0:T(8,128)(2,1)S(1)} %shard_map.172) | data formatting | bytes 524288

commit v2 on v1

--- a/solution.py
+++ b/solution.py
@@ -12,6 +12,8 @@
 WINDOW_SHIFT = 0.05
 LEAF = 128
 CHUNK = 16
+PIECE = 64
+EXACT = False
 MESH = pl.DeviceIdType.MESH
 F32 = jnp.float32
 BF16 = jnp.bfloat16
@@ -56,8 +58,8 @@
     both = np.zeros((seq, 2 * hidden))
     both[:, :features] = feats(np.arange(seq))
     both[:, hidden : hidden + features] = feats(seq - np.arange(seq))
-    fhi, flo = split_np(both)
-    return fcat, gcat, twist, fhi, flo
+    feat = np.concatenate(split_np(both), axis=1)
+    return fcat, gcat, twist, feat
 
 
 def split(x):
@@ -69,8 +71,9 @@
     return jnp.dot(a, b, preferred_element_type=F32)
 
 
-def dot3(a, b):
-    return dot(a[0], b[0]) + dot(a[1], b[0]) + dot(a[0], b[1])
+def deep(a, b):
+    half = b.shape[0] // 2
+    return dot(a[:, :half], b[:half]) + dot(a[:, half:], b[half:])
 
 
 PI_A = 3.140625
@@ -130,16 +133,17 @@
 
 def kernel(
     sizes,
-    tok_h, wv_h, wa_h, wb_h, fcat_h, gcat_h, twist_h, fhi_h, flo_h,
+    tok_h, wv_h, wa_h, wb_h, fcat_h, gcat_h, twist_h, feat_h,
     wf_h, own_taps_h, gate_taps_h, pw_h, pb_h, sf_h, hw_h, hb_h, fb_h, ld_h,
     out_ref,
     own_taps, gate_taps, pw, pb, sf, hw, hb, fb, ld,
-    tok, wva, wb, fcat, gcat, twist, fhi, flo,
-    wf, sbuf, rbuf, gb, halo, pad, xs, gs, gpad, gbs,
-    pwb, hwb, wfb, kre, kim, xhi, xlo, spec, ybuf, s2, r2,
+    tok, acc, wva, wb, fcat, gcat, twist, feat,
+    wf, sbuf, rbuf, gb, halo, pad, xs, gpad, gbs,
+    pwb, hwb, w1, w2, w3, kre, kim, xhi, xlo, spec, ybuf, s2, r2,
     in_sem, send_sem, recv_sem, halo_send, halo_recv, back_send, back_recv,
 ):
     R, T, N, C, S, HID, PE = sizes
+    D = tok.shape[1]
     L = N // LEAF
     row = lax.axis_index("row")
     col = lax.axis_index("col")
@@ -152,23 +156,29 @@
 
     half = R // 2
     H = S // 2
-    far = 1 - row // half
-    order = [far, 1 - far]
+    low = row < half
+    inner = jnp.logical_and(row > 0, row < R - 1)
+    first = lax.rem(row, half)
+    far = [jnp.where(low, half + i, half - 1 - i) for i in range(half)]
+    near = [jnp.where(low, 0, half) + lax.rem(first + i, half) for i in range(1, half)]
+    order = [jnp.where(low, 1, 0), jnp.where(low, 0, 1)]
 
     def load(i, src, dst):
         copy = pltpu.make_async_copy(src, dst, in_sem.at[i])
         copy.start()
         return copy
 
-    def load_half(i, src, which, k):
+    def load_half(i, src, which, k, rows=slice(None)):
         lanes = pl.ds(pl.multiple_of(order[k] * H, H), H)
-        return load(i, src.at[:, lanes], wva.at[k, :, which * H : (which + 1) * H])
-
-    ld_tok = load(0, tok_h, tok)
-    ld_half = [
-        [load_half(2 * k + which + 1, src, which, k) for which, src in enumerate((wv_h, wa_h))]
-        for k in range(2)
-    ]
+        return load(i, src.at[rows, lanes], wva.at[k, rows, which * H : (which + 1) * H])
+
+    halves = [slice(0, D // 2), slice(D // 2, D)]
+    ld_first = []
+    for i, part in enumerate(halves):
+        ld_first.append([
+            load(2 * i, tok_h.at[:, part], tok.at[:, part]),
+            load_half(2 * i + 1, wv_h, 0, 0, part),
+        ])
 
     barrier = pltpu.get_barrier_semaphore()
     peers = [lax.rem(row + d, R) for d in range(R)]
@@ -176,16 +186,19 @@
     for d in range(1, R):
         pl.semaphore_signal(barrier, inc=1, device_id={"row": peers[d]}, device_id_type=MESH)
 
-    def out_copy(which, target, slot):
+    def pieces(total, size):
+        return [pl.ds(at, size) for at in range(0, total, size)]
+
+    def out_copy(which, target, slot, part):
         return pltpu.make_async_remote_copy(
-            src_ref=sbuf.at[which, target], dst_ref=rbuf.at[which, row],
+            src_ref=sbuf.at[which, target, part], dst_ref=rbuf.at[which, row, part],
             send_sem=send_sem.at[which, slot], recv_sem=recv_sem.at[which, row],
             device_id={"row": target}, device_id_type=MESH)
 
     def in_copy(which, d):
         return pltpu.make_async_remote_copy(
             src_ref=sbuf.at[which, peers[d]], dst_ref=rbuf.at[which, sources[d]],
-            send_sem=send_sem.at[which, d], recv_sem=recv_sem.at[which, sources[d]],
+            send_sem=send_sem.at[which, d - 1], recv_sem=recv_sem.at[which, sources[d]],
             device_id={"row": peers[d]}, device_id_type=MESH)
 
     def halo_copy(side):
@@ -196,80 +209,108 @@
             send_sem=halo_send.at[side], recv_sem=halo_recv.at[side],
             device_id={"row": target}, device_id_type=MESH)
 
-    def back_out(d):
+    def back_out(j, part):
+        a, b = (far + near)[j], (near + far)[j]
+        target = jnp.where(inner, a, b)
         return pltpu.make_async_remote_copy(
-            src_ref=s2.at[peers[d]], dst_ref=r2.at[row],
-            send_sem=back_send.at[d], recv_sem=back_recv.at[d],
-            device_id={"row": peers[d]}, device_id_type=MESH)
+            src_ref=s2.at[target, part], dst_ref=r2.at[row, part],
+            send_sem=back_send.at[j], recv_sem=back_recv.at[row],
+            device_id={"row": target}, device_id_type=MESH)
 
     def back_in(d):
         return pltpu.make_async_remote_copy(
             src_ref=s2.at[peers[d]], dst_ref=r2.at[sources[d]],
-            send_sem=back_send.at[d], recv_sem=back_recv.at[d],
+            send_sem=back_send.at[d - 1], recv_sem=back_recv.at[sources[d]],
             device_id={"row": peers[d]}, device_id_type=MESH)
 
-    ld_tok.wait()
-    sends = []
-    first = lax.rem(row, half)
-
     def send(which, k):
-        for i in range(k, half):
-            target = order[k] * half + lax.rem(first + i, half)
-            copy = out_copy(which, target, k * half + i)
-            copy.start()
-            sends.append(copy)
-
-    for k in range(2):
-        for copy in ld_half[k]:
-            copy.wait()
-        if k == 0:
-            ld_wb = load(5, wb_h, wb)
-            ld_fhi, ld_flo = load(6, fhi_h, fhi), load(7, flo_h, flo)
-            small = [
-                load(12 + i, src, dst)
-                for i, (src, dst) in enumerate([
-                    (own_taps_h, own_taps), (gate_taps_h, gate_taps), (pw_h, pw), (pb_h, pb),
-                    (sf_h, sf), (hw_h, hw), (hb_h, hb), (fb_h, fb), (ld_h, ld)])
-            ]
-        made = dot(tok[...], wva[k]).astype(BF16)
-        for which in range(2):
-            for i in range(half):
-                base = which * H + i * C
-                sbuf[which, order[k] * half + i] = made[:, base : base + C]
-        if k == 0:
-            pl.semaphore_wait(barrier, R - 1)
-            send(0, 0)
-    send(0, 1)
-    send(1, 0)
-    send(1, 1)
-    for which in range(2):
-        rbuf[which, row] = sbuf[which, row]
+        for slot, target in enumerate(near if k else far):
+            for part in pieces(T, min(PIECE, T)):
+                out_copy(which, target, slot + (half if k else 0), part).start()
+
+    def keep(which, k, made):
+        for i in range(half):
+            sbuf[which, order[k] * half + i] = made[:, i * C : (i + 1) * C]
+
+    for copy in ld_first[0]:
+        copy.wait()
+    ld_near = [load_half(5 + which, src, which, 1) for which, src in enumerate((wv_h, wa_h))]
+    ld_far_a = load_half(4, wa_h, 1, 0)
+    small = [
+        load(12 + i, src, dst)
+        for i, (src, dst) in enumerate([
+            (own_taps_h, own_taps), (gate_taps_h, gate_taps), (pw_h, pw), (pb_h, pb),
+            (sf_h, sf), (hw_h, hw), (hb_h, hb), (fb_h, fb), (ld_h, ld)])
+    ]
     if aligned:
         wf_src = wf_h.at[:, :, :, pl.ds(pl.multiple_of(row * C, 128), C)]
     else:
         wf_src = wf_h
     ld_wf = load(8, wf_src, wf)
+    ld_wb = load(7, wb_h, wb)
+    ld_feat = load(21, feat_h, feat)
+    acc[...] = deep(tok[:, halves[0]], wva[0, halves[0], 0:H])
+    for copy in ld_first[1]:
+        copy.wait()
+    acc[...] += deep(tok[:, halves[1]], wva[0, halves[1], 0:H])
+    keep(0, 0, acc[...].astype(BF16))
+
+    @pl.when(inner)
+    def _():
+        pl.semaphore_wait(barrier, R - 1)
+        send(0, 0)
+
+    for copy in ld_near:
+        copy.wait()
+    made = dot(tok[...], wva[1]).astype(BF16)
+    keep(0, 1, made[:, 0:H])
+    keep(1, 1, made[:, H : 2 * H])
+
+    @pl.when(jnp.logical_not(inner))
+    def _():
+        pl.semaphore_wait(barrier, R - 1)
+        send(0, 1)
+        send(0, 0)
+
+    ld_far_a.wait()
+    keep(1, 0, deep(tok[...], wva[0, :, H : 2 * H]).astype(BF16))
+
+    @pl.when(inner)
+    def _():
+        send(1, 0)
+        send(0, 1)
+        send(1, 1)
+
+    @pl.when(jnp.logical_not(inner))
+    def _():
+        send(1, 1)
+        send(1, 0)
+
+    for which in range(2):
+        rbuf[which, row] = sbuf[which, row]
     ld_fcat, ld_twist, ld_gcat = load(9, fcat_h, fcat), load(10, twist_h, twist), load(11, gcat_h, gcat)
-    ld_wb.wait()
-    gb[...] = dot(tok[...], wb[...]).astype(BF16)
-    for side in range(2):
-        halo_copy(side).start()
-
     for copy in small:
         copy.wait()
+    W = 2 * HID
     pwb[...] = jnp.zeros_like(pwb)
     pwb[0:PE, 0:HID] = pw[...]
     pwb[HID : HID + PE, HID : 2 * HID] = pw[...]
     hwb[...] = jnp.zeros_like(hwb)
     hwb[0:HID, 0:HID] = hw[...]
     hwb[HID : 2 * HID, HID : 2 * HID] = hw[...]
-    wfb[...] = jnp.zeros_like(wfb)
+    for w, full in ((w1, pwb), (w2, hwb)):
+        high, low = split(full[...])
+        w[0:W, 0:W] = high
+        w[0:W, W : 2 * W] = low
+        w[W : 2 * W, 0:W] = high
+        w[W : 2 * W, W : 2 * W] = jnp.zeros_like(low)
     ld_wf.wait()
     for o in range(2):
-        wfb[0:HID, o * C : (o + 1) * C] = wf[:, o, 0, :]
-        wfb[HID : 2 * HID, (2 + o) * C : (3 + o) * C] = wf[:, o, 1, :]
-    ld_fhi.wait()
-    ld_flo.wait()
+        for way in range(2):
+            high, low = split(wf[:, o, way, :])
+            for at, part in enumerate((high, high, low, low)):
+                w3[way, at * HID : (at + 1) * HID, o * C : (o + 1) * C] = part
+    ld_feat.wait()
 
     def twice(v):
         return jnp.concatenate([v, v], axis=-1)
@@ -280,22 +321,27 @@
 
     def filter_rows(step, carry):
         at = pl.ds(pl.multiple_of(step * rows_f, rows_f), rows_f)
-        pre = dot3((fhi[at, :], flo[at, :]), split(pwb[...])) + pb2
-        ha = sine(sf2[0:1] * pre)
-        pre = dot3(split(ha), split(hwb[...])) + hb2
-        hb_ = sine(sf2[1:2] * pre)
-        raw = dot3(split(hb_), split(wfb[...]))
+        both = dot(feat[at, :], w1[...])
+        ha = sine(sf2[0:1] * (both[:, 0:W] + both[:, W : 2 * W] + pb2))
+        both = dot(jnp.concatenate(split(ha), axis=-1), w2[...])
+        hb_ = sine(sf2[1:2] * (both[:, 0:W] + both[:, W : 2 * W] + hb2))
+        swapped = pltpu.roll(hb_, HID, 1)
+        lower = lax.broadcasted_iota(jnp.int32, (rows_f, W), 1) < HID
+        raw = []
+        for way, (head, tail) in enumerate(((hb_, swapped), (swapped, hb_))):
+            part = jnp.where(lower, head, tail - tail.astype(BF16).astype(F32)).astype(BF16)
+            raw.append(dot(jnp.concatenate([part, part], axis=-1), w3[way]))
         index = (lax.broadcasted_iota(jnp.int32, (rows_f, C), 0) + step * rows_f).astype(F32)
         scale = 1.0 / max(N - 1, 1)
         env_f = jnp.exp(-(index * scale) * decay) + WINDOW_SHIFT
         env_b = jnp.exp(-((N - index) * scale) * decay) + WINDOW_SHIFT
         env_b = jnp.where(index > 0.0, -env_b, 0.0)
         for o in range(2):
-            kre[o, at, :] = raw[:, o * C : (o + 1) * C] * env_f
-            kim[o, at, :] = raw[:, (2 + o) * C : (3 + o) * C] * env_b
+            kre[o, at, :] = raw[0][:, o * C : (o + 1) * C] * env_f
+            kim[o, at, :] = raw[1][:, o * C : (o + 1) * C] * env_b
         return carry
 
-    lax.fori_loop(0, N // rows_f, filter_rows, 0)
+    lax.fori_loop(0, N // rows_f, filter_rows, 0, unroll=2)
     ld_fcat.wait()
     ld_twist.wait()
     ld_gcat.wait()
@@ -340,13 +386,16 @@
         def kernel_in(step, carry, o=o):
             at = step * CHUNK
             blocks = [(kre[o, rows_at(n1, at), :], kim[o, rows_at(n1, at), :]) for n1 in range(L)]
-            put_leaves(split_tree(blocks, math.pi / 2), at, True)
+            put_leaves(split_tree(blocks, math.pi / 2), at, EXACT)
             return carry
 
         lax.fori_loop(0, steps, kernel_in, 0)
         for tile in range(L * C // width):
             lanes = slice(tile * width, (tile + 1) * width)
-            spec[o, :, lanes] = mul3(fcat, xhi[:, lanes], xlo[:, lanes])
+            if EXACT:
+                spec[o, :, lanes] = mul3(fcat, xhi[:, lanes], xlo[:, lanes])
+            else:
+                spec[o, :, lanes] = dot(fcat[0:K2], xhi[:, lanes])
 
     def through(o, exact):
         for tile in range(L * C // width):
@@ -363,9 +412,7 @@
             else:
                 ybuf[:, lanes] = dot(gcat[0:K2], y.astype(BF16))
 
-    def short(which, dest):
-        for d in range(1, R):
-            in_copy(which, d).wait_recv()
+    def short(which):
         pad[0:8] = jnp.zeros((8, C), F32)
         pad[8 + N : 16 + N] = jnp.zeros((8, C), F32)
         for r in range(R):
@@ -373,38 +420,48 @@
         taps = own_taps[which, :, own_at].astype(F32)
         for r in range(R):
             a = r * T
-            dest[a : a + T] = (
+            made = (
                 taps[0:1] * pad[7 + a : 7 + a + T]
                 + taps[1:2] * pad[8 + a : 8 + a + T]
                 + taps[2:3] * pad[9 + a : 9 + a + T]
             ).astype(BF16).astype(F32)
-
-    short(0, xs)
+            xs[a : a + T] = made if which == 0 else made * xs[a : a + T]
+
+    for d in range(1, R):
+        in_copy(0, d).wait_recv()
+
+    short(0)
     bias = fb[:, own_at]
 
-    def value_in(step, carry):
-        at = step * CHUNK
-        blocks = [(xs[rows_at(n1, at), :], None) for n1 in range(L)]
-        put_leaves(split_tree(blocks, math.pi / 2), at, True)
-        return carry
-
-    lax.fori_loop(0, steps, value_in, 0)
-    through(0, True)
-    short(1, gs)
+    def signal_in(exact):
+        def body(step, carry):
+            at = step * CHUNK
+            blocks = [(xs[rows_at(n1, at), :], None) for n1 in range(L)]
+            put_leaves(split_tree(blocks, math.pi / 2), at, exact)
+            return carry
+
+        lax.fori_loop(0, steps, body, 0)
+
+    signal_in(EXACT)
+    through(0, EXACT)
 
     def middle(step, carry):
         at = step * CHUNK
         convolved = join_tree(get_leaves(at), math.pi / 2, True)
-        blocks = []
         for n1 in range(L):
             here = rows_at(n1, at)
-            gated = gs[here, :] * (convolved[n1] + bias[0:1] * xs[here, :])
-            xs[here, :] = gated
-            blocks.append((gated, None))
-        put_leaves(split_tree(blocks, math.pi / 2), at, False)
+            xs[here, :] = convolved[n1] + bias[0:1] * xs[here, :]
         return carry
 
     lax.fori_loop(0, steps, middle, 0)
+    ld_wb.wait()
+    gb[...] = dot(tok[...], wb[...]).astype(BF16)
+    for side in range(2):
+        halo_copy(side).start()
+    for d in range(1, R):
+        in_copy(1, d).wait_recv()
+    short(1)
+    signal_in(False)
     through(1, False)
 
     def last(step, carry):
@@ -416,9 +473,11 @@
             s2[r, pl.ds(pl.multiple_of(inner + at, CHUNK), CHUNK), :] = value.astype(BF16)
         return carry
 
-    lax.fori_loop(0, steps, last, 0)
-    for d in [half] + [d for d in range(1, R) if d != half]:
-        back_out(d).start()
+    for part in range(2):
+        lax.fori_loop(part * steps // 2, (part + 1) * steps // 2, last, 0)
+        for j in range(R - 1):
+            for n1 in range(T // LEAF):
+                back_out(j, pl.ds(n1 * LEAF + part * LEAF // 2, LEAF // 2)).start()
     r2[row] = s2[row]
 
     for side in range(2):
@@ -437,10 +496,10 @@
     for r in range(R):
         lanes = slice(r * C, (r + 1) * C)
         out_ref[:, lanes] = (gbs[:, lanes] * r2[r].astype(F32)).astype(BF16)
-    for copy in sends:
-        copy.wait_send()
     for d in range(1, R):
-        back_out(d).wait_send()
+        for which in range(2):
+            in_copy(which, d).wait_send()
+        back_in(d).wait_send()
     for side in range(2):
         halo_copy(side).wait_send()
 
@@ -457,7 +516,7 @@
     PE, HID = pos_weight.shape
     L = N // LEAF
     row, col = lax.axis_index("row"), lax.axis_index("col")
-    fcat, gcat, twist, fhi, flo = tables(N, C, PE, HID)
+    fcat, gcat, twist, feat = tables(N, C, PE, HID)
     own_w = filter_out
     own_taps, gate_taps, fb, ld = short_taps, short_taps, filter_bias, lag_decay[None]
     if C % 128:
@@ -474,17 +533,17 @@
     return pl.pallas_call(
         functools.partial(kernel, (R, T, N, C, S, HID, PE)),
         out_shape=jax.ShapeDtypeStruct((T, S), BF16),
-        in_specs=[hbm] * 19,
+        in_specs=[hbm] * 18,
         out_specs=vm,
         scratch_shapes=[pltpu.VMEM(x.shape, x.dtype) for x in small] + [
             pltpu.VMEM((T, D), BF16),
+            pltpu.VMEM((T, S // 2), F32),
             pltpu.VMEM((2, D, S), BF16),
             pltpu.VMEM((D, S), BF16),
             pltpu.VMEM(fcat.shape, BF16),
             pltpu.VMEM(gcat.shape, BF16),
             pltpu.VMEM(twist.shape, F32),
-            pltpu.VMEM(fhi.shape, BF16),
-            pltpu.VMEM(flo.shape, BF16),
+            pltpu.VMEM(feat.shape, BF16),
             pltpu.VMEM((HID, 2, 2, C), F32),
             pltpu.VMEM((2, R, T, C), BF16),
             pltpu.VMEM((2, R, T, C), BF16),
@@ -492,12 +551,13 @@
             pltpu.VMEM((2, CHUNK, S), BF16),
             pltpu.VMEM((N + 16, C), F32),
             pltpu.VMEM((N, C), F32),
-            pltpu.VMEM((N, C), F32),
             pltpu.VMEM((T + 16, S), F32),
             pltpu.VMEM((T, S), F32),
             pltpu.VMEM((2 * HID, 2 * HID), F32),
             pltpu.VMEM((2 * HID, 2 * HID), F32),
-            pltpu.VMEM((2 * HID, 4 * C), F32),
+            pltpu.VMEM((4 * HID, 4 * HID), BF16),
+            pltpu.VMEM((4 * HID, 4 * HID), BF16),
+            pltpu.VMEM((2, 4 * HID, 2 * C), BF16),
             pltpu.VMEM((2, N, C), F32),
             pltpu.VMEM((2, N, C), F32),
             pltpu.VMEM((2 * LEAF, L * C), BF16),
@@ -506,7 +566,7 @@
             pltpu.VMEM((2 * LEAF, L * C), F32),
             pltpu.VMEM((R, T, C), BF16),
             pltpu.VMEM((R, T, C), BF16),
-            dma((21,)),
+            dma((22,)),
             dma((2, R)),
             dma((2, R)),
             dma((2,)),
@@ -519,7 +579,7 @@
         ),
     )(*[
         pltpu.with_memory_space_constraint(jnp.asarray(x), pltpu.HBM)
-        for x in (tokens, w_value, w_gate_a, w_gate_b, fcat, gcat, twist, fhi, flo, own_w, *small)
+        for x in (tokens, w_value, w_gate_a, w_gate_b, fcat, gcat, twist, feat, own_w, *small)
     ])
 
 

time: 27 us -> 26.8 us (level)
  no operation moved by 1% of the time
where the time goes in v2:
time: 26.8 us; the launch traced here: 26.7 us
  Pallas kernels  26 us (97%)
  local copies, waits for them, and re-layouts  0.71 us (3%)
    pallas_call x1, Pallas kernels, per_device(): pl.pallas_call(functools.partial(kernel, (R, T, N, C, S, HID, PE)), out_s...  26 us
    unnamed x1, local copies, waits for them, and re-layouts  0.71 us

profile of v2, /device:TPU:0, one launch (start us, length us, event | category | flops | bytes accessed | tf_op | source)
XLA Modules:
  0.0 26.7 jit_solution(5231464686573204956)
XLA Ops:
  0.0 26.0 %shard_map.163 = bf16[256,512]{1,0:T(8,128)(2,1)S(1)} custom-call(bf16[256,2048]{1,0:T(8,128)(2,1)} %tok_h.1, bf16[2048,512]{1,0:T(8,128)(2,1)} %wv_h.1, bf16[2048,512]{1,0:T(8,128)(2,1)} %wa_h.1, bf16[2048,512]{1,0:T(8,128)(2,1)} %wb_h.1, bf16[512,256]{1,0:T(8,128)(2,1)} %constant.8.clone.fcat_h, bf16[512,256]{1,0:T(8,128)(2,1)} %constant.9.clone.gcat_h, ...), custom_call_target="tpu_custom_call" | custom-call | tf_op jit(solution)/shard_map/pallas_call | solution.py:533
  26.0 0.7 %copy.19 = bf16[256,512]{1,0:T(8,128)(2,1)} copy(bf16[256,512]{1,0:T(8,128)(2,1)S(1)} %shard_map.163) | data formatting | bytes 524288

commit v3 on v2

--- a/solution.py
+++ b/solution.py
@@ -12,7 +12,7 @@
 WINDOW_SHIFT = 0.05
 LEAF = 128
 CHUNK = 16
-PIECE = 64
+PIECE = 256
 EXACT = False
 MESH = pl.DeviceIdType.MESH
 F32 = jnp.float32
@@ -210,8 +210,7 @@
             device_id={"row": target}, device_id_type=MESH)
 
     def back_out(j, part):
-        a, b = (far + near)[j], (near + far)[j]
-        target = jnp.where(inner, a, b)
+        target = (far + near)[j]
         return pltpu.make_async_remote_copy(
             src_ref=s2.at[target, part], dst_ref=r2.at[row, part],
             send_sem=back_send.at[j], recv_sem=back_recv.at[row],
@@ -277,11 +276,10 @@
 
     @pl.when(inner)
     def _():
-        send(1, 0)
         send(0, 1)
-        send(1, 1)
-
-    @pl.when(jnp.logical_not(inner))
+
+    even = lax.rem(col, 2) == 0
+    @pl.when(even)
     def _():
         send(1, 1)
         send(1, 0)
@@ -429,6 +427,11 @@
 
     for d in range(1, R):
         in_copy(0, d).wait_recv()
+
+    @pl.when(jnp.logical_not(even))
+    def _():
+        send(1, 1)
+        send(1, 0)
 
     short(0)
     bias = fb[:, own_at]

time: 26.8 us -> 25.6 us (0.955)
  the two profiles are of different devices: /device:TPU:0 before, /device:TPU:1 now
where the time goes in v3:
time: 25.6 us; the launch traced here: 25.4 us
  Pallas kernels  24.7 us (96%)
  local copies, waits for them, and re-layouts  0.71 us (3%)
    pallas_call x1, Pallas kernels, per_device(): pl.pallas_call(functools.partial(kernel, (R, T, N, C, S, HID, PE)), out_s...  24.7 us
    unnamed x1, local copies, waits for them, and re-layouts  0.71 us

profile of v3, /device:TPU:1, one launch (start us, length us, event | category | flops | bytes accessed | tf_op | source)
XLA Modules:
  0.0 25.4 jit_solution(12786096786791117460)
XLA Ops:
  0.0 24.7 %shard_map.163 = bf16[256,512]{1,0:T(8,128)(2,1)S(1)} custom-call(bf16[256,2048]{1,0:T(8,128)(2,1)} %tok_h.1, bf16[2048,512]{1,0:T(8,128)(2,1)} %wv_h.1, bf16[2048,512]{1,0:T(8,128)(2,1)} %wa_h.1, bf16[2048,512]{1,0:T(8,128)(2,1)} %wb_h.1, bf16[512,256]{1,0:T(8,128)(2,1)} %constant.8.clone.fcat_h, bf16[512,256]{1,0:T(8,128)(2,1)} %constant.9.clone.gcat_h, ...), custom_call_target="tpu_custom_call" | custom-call | tf_op jit(solution)/shard_map/pallas_call | solution.py:536
  24.7 0.7 %copy.19 = bf16[256,512]{1,0:T(8,128)(2,1)} copy(bf16[256,512]{1,0:T(8,128)(2,1)S(1)} %shard_map.163) | data formatting | bytes 524288

commit v4 on v3

--- a/solution.py
+++ b/solution.py
@@ -71,9 +71,11 @@
     return jnp.dot(a, b, preferred_element_type=F32)
 
 
-def deep(a, b):
+def deep(acc, a, b, add=False):
     half = b.shape[0] // 2
-    return dot(a[:, :half], b[:half]) + dot(a[:, half:], b[half:])
+    for i, part in enumerate((slice(0, half), slice(half, None))):
+        made = dot(a[:, part], b[part])
+        acc[i] = acc[i] + made if add else made
 
 
 PI_A = 3.140625
@@ -157,7 +159,7 @@
     half = R // 2
     H = S // 2
     low = row < half
-    inner = jnp.logical_and(row > 0, row < R - 1)
+    inner = row > 0
     first = lax.rem(row, half)
     far = [jnp.where(low, half + i, half - 1 - i) for i in range(half)]
     near = [jnp.where(low, 0, half) + lax.rem(first + i, half) for i in range(1, half)]
@@ -209,10 +211,10 @@
             send_sem=halo_send.at[side], recv_sem=halo_recv.at[side],
             device_id={"row": target}, device_id_type=MESH)
 
-    def back_out(j, part):
-        target = (far + near)[j]
+    def back_out(j):
+        target = (far[::-1] + near)[j]
         return pltpu.make_async_remote_copy(
-            src_ref=s2.at[target, part], dst_ref=r2.at[row, part],
+            src_ref=s2.at[target], dst_ref=r2.at[row],
             send_sem=back_send.at[j], recv_sem=back_recv.at[row],
             device_id={"row": target}, device_id_type=MESH)
 
@@ -248,11 +250,11 @@
     ld_wf = load(8, wf_src, wf)
     ld_wb = load(7, wb_h, wb)
     ld_feat = load(21, feat_h, feat)
-    acc[...] = deep(tok[:, halves[0]], wva[0, halves[0], 0:H])
+    deep(acc, tok[:, halves[0]], wva[0, halves[0], 0:H])
     for copy in ld_first[1]:
         copy.wait()
-    acc[...] += deep(tok[:, halves[1]], wva[0, halves[1], 0:H])
-    keep(0, 0, acc[...].astype(BF16))
+    deep(acc, tok[:, halves[1]], wva[0, halves[1], 0:H], True)
+    keep(0, 0, (acc[0] + acc[1]).astype(BF16))
 
     @pl.when(inner)
     def _():
@@ -272,7 +274,8 @@
         send(0, 0)
 
     ld_far_a.wait()
-    keep(1, 0, deep(tok[...], wva[0, :, H : 2 * H]).astype(BF16))
+    deep(acc, tok[...], wva[0, :, H : 2 * H])
+    keep(1, 0, (acc[0] + acc[1]).astype(BF16))
 
     @pl.when(inner)
     def _():
@@ -428,11 +431,6 @@
     for d in range(1, R):
         in_copy(0, d).wait_recv()
 
-    @pl.when(jnp.logical_not(even))
-    def _():
-        send(1, 1)
-        send(1, 0)
-
     short(0)
     bias = fb[:, own_at]
 
@@ -457,6 +455,11 @@
         return carry
 
     lax.fori_loop(0, steps, middle, 0)
+    @pl.when(jnp.logical_not(even))
+    def _():
+        send(1, 1)
+        send(1, 0)
+
     ld_wb.wait()
     gb[...] = dot(tok[...], wb[...]).astype(BF16)
     for side in range(2):
@@ -476,11 +479,9 @@
             s2[r, pl.ds(pl.multiple_of(inner + at, CHUNK), CHUNK), :] = value.astype(BF16)
         return carry
 
-    for part in range(2):
-        lax.fori_loop(part * steps // 2, (part + 1) * steps // 2, last, 0)
-        for j in range(R - 1):
-            for n1 in range(T // LEAF):
-                back_out(j, pl.ds(n1 * LEAF + part * LEAF // 2, LEAF // 2)).start()
+    lax.fori_loop(0, steps, last, 0)
+    for j in range(R - 1):
+        back_out(j).start()
     r2[row] = s2[row]
 
     for side in range(2):
@@ -540,7 +541,7 @@
         out_specs=vm,
         scratch_shapes=[pltpu.VMEM(x.shape, x.dtype) for x in small] + [
             pltpu.VMEM((T, D), BF16),
-            pltpu.VMEM((T, S // 2), F32),
+            pltpu.VMEM((2, T, S // 2), F32),
             pltpu.VMEM((2, D, S), BF16),
             pltpu.VMEM((D, S), BF16),
             pltpu.VMEM(fcat.shape, BF16),

time: 25.6 us -> 23.9 us (0.934)
  Pallas kernels: 24.7 us -> 23.1 us
    pallas_call x1, Pallas kernels: 24.7 us -> 23.1 us  [per_device(): pl.pallas_call(functools.partial(kernel, (R, T, N, C, S, HID, PE)), out_s...]
where the time goes in v4:
time: 23.9 us; the launch traced here: 23.8 us
  Pallas kernels  23.1 us (97%)
  local copies, waits for them, and re-layouts  0.71 us (3%)
    pallas_call x1, Pallas kernels, per_device(): pl.pallas_call(functools.partial(kernel, (R, T, N, C, S, HID, PE)), out_s...  23.1 us
    unnamed x1, local copies, waits for them, and re-layouts  0.71 us

profile of v4, /device:TPU:1, one launch (start us, length us, event | category | flops | bytes accessed | tf_op | source)
XLA Modules:
  0.0 23.8 jit_solution(14900364907401323075)
XLA Ops:
  0.0 23.1 %shard_map.163 = bf16[256,512]{1,0:T(8,128)(2,1)S(1)} custom-call(bf16[256,2048]{1,0:T(8,128)(2,1)} %tok_h.1, bf16[2048,512]{1,0:T(8,128)(2,1)} %wv_h.1, bf16[2048,512]{1,0:T(8,128)(2,1)} %wa_h.1, bf16[2048,512]{1,0:T(8,128)(2,1)} %wb_h.1, bf16[512,256]{1,0:T(8,128)(2,1)} %constant.8.clone.fcat_h, bf16[512,256]{1,0:T(8,128)(2,1)} %constant.9.clone.gcat_h, ...), custom_call_target="tpu_custom_call" | custom-call | tf_op jit(solution)/shard_map/pallas_call | solution.py:537
  23.1 0.7 %copy.19 = bf16[256,512]{1,0:T(8,128)(2,1)} copy(bf16[256,512]{1,0:T(8,128)(2,1)S(1)} %shard_map.163) | data formatting | bytes 524288

commit v5 on v4

--- a/solution.py
+++ b/solution.py
@@ -212,7 +212,7 @@
             device_id={"row": target}, device_id_type=MESH)
 
     def back_out(j):
-        target = (far[::-1] + near)[j]
+        target = jnp.where(row == 0, (near + far[::-1])[j], (far[::-1] + near)[j])
         return pltpu.make_async_remote_copy(
             src_ref=s2.at[target], dst_ref=r2.at[row],
             send_sem=back_send.at[j], recv_sem=back_recv.at[row],

time: 23.9 us -> 23.9 us (level)
  no operation moved by 1% of the time
where the time goes in v5:
time: 23.9 us; the launch traced here: 23.8 us
  Pallas kernels  23.1 us (97%)
  local copies, waits for them, and re-layouts  0.71 us (3%)
    pallas_call x1, Pallas kernels, per_device(): pl.pallas_call(functools.partial(kernel, (R, T, N, C, S, HID, PE)), out_s...  23.1 us
    unnamed x1, local copies, waits for them, and re-layouts  0.71 us

profile of v5, /device:TPU:1, one launch (start us, length us, event | category | flops | bytes accessed | tf_op | source)
XLA Modules:
  0.0 23.8 jit_solution(2083791143952718307)
XLA Ops:
  0.0 23.1 %shard_map.163 = bf16[256,512]{1,0:T(8,128)(2,1)S(1)} custom-call(bf16[256,2048]{1,0:T(8,128)(2,1)} %tok_h.1, bf16[2048,512]{1,0:T(8,128)(2,1)} %wv_h.1, bf16[2048,512]{1,0:T(8,128)(2,1)} %wa_h.1, bf16[2048,512]{1,0:T(8,128)(2,1)} %wb_h.1, bf16[512,256]{1,0:T(8,128)(2,1)} %constant.8.clone.fcat_h, bf16[512,256]{1,0:T(8,128)(2,1)} %constant.9.clone.gcat_h, ...), custom_call_target="tpu_custom_call" | custom-call | tf_op jit(solution)/shard_map/pallas_call | solution.py:537
  23.1 0.7 %copy.19 = bf16[256,512]{1,0:T(8,128)(2,1)} copy(bf16[256,512]{1,0:T(8,128)(2,1)S(1)} %shard_map.163) | data formatting | bytes 524288
